TPU v7x, 32 devices: a whole 2x2x4 slice. The times are simulated.
32 devices in a mesh: fs: 8 (over z, y), tp: 4 (over x, core).
Axes of the slice: x: 2, y: 2, z: 4, core: 2. Of those that a mesh axis runs over, the one named last changes fastest.
Arguments:
- x_saved: bfloat16 [16384, 2048], P('fs'), may hold values from -6 to 6
- h_saved: bfloat16 [16384, 1024], P('fs', 'tp'), may hold values from -6 to 6
- key_cot: bfloat16 [16384, 1024], P('fs', 'tp'), may hold values from -6 to 6
- value_cot: bfloat16 [16384, 1024], P('fs', 'tp'), may hold values from -6 to 6
- out_cot: bfloat16 [16384, 2048], P('fs'), may hold values from -6 to 6
- w_key: float32 [2048, 1024], P('fs', 'tp'), may hold values from -0.125 to 0.125
- w_value: float32 [2048, 1024], P('fs', 'tp'), may hold values from -0.125 to 0.125
- w_out: float32 [1024, 2048], P('tp', 'fs'), may hold values from -0.1875 to 0.1875
- p_key: bfloat16 [2048, 256], P('fs'), may hold values from -1 to 1, as said below
- p_value: bfloat16 [2048, 256], P('fs'), may hold values from -1 to 1, as said below
- p_out: bfloat16 [2048, 256], P('fs'), may hold values from -1 to 1, as said below
- m_key: float32 [2, 256, 1024], P(None, 'fs', 'tp'), may hold values from -1.5 to 1.5, as said below
- m_value: float32 [2, 256, 1024], P(None, 'fs', 'tp'), may hold values from -1.5 to 1.5, as said below
- m_out: float32 [2, 256, 1024], P(None, 'fs', 'tp'), may hold values from -1.5 to 1.5, as said below
Outputs:
- step_key: float32 [2048, 1024], P('fs', 'tp')
- step_value: float32 [2048, 1024], P('fs', 'tp')
- step_out: float32 [1024, 2048], P('tp', 'fs')
- copy_key: bfloat16 [2048, 1024], P(None, 'tp')
- copy_value: bfloat16 [2048, 1024], P(None, 'tp')
- copy_out: bfloat16 [1024, 2048], P('tp')
- new_m_key: float32 [2, 256, 1024], P(None, 'fs', 'tp')
- new_m_value: float32 [2, 256, 1024], P(None, 'fs', 'tp')
- new_m_out: float32 [2, 256, 1024], P(None, 'fs', 'tp')
Inputs may be any that keep to these rules, and one draw needn't show every extreme that they name: `p_key`: factor entries are real-valued, dense and of full rank. `p_value`: factor entries are real-valued, dense and of full rank. `p_out`: factor entries are real-valued, dense and of full rank. `m_key`: plane 1 (second moments) lies in 0.05 to 1. `m_value`: plane 1 (second moments) lies in 0.05 to 1. `m_out`: plane 1 (second moments) lies in 0.05 to 1.
All inputs are finite; a program needn't handle non-finite values.
Results may differ from a plain program's by a relative error of at most 0.0085.
Values may be sent and summed in bfloat16 or wider, within the bound.
A program may use at most 128 MiB of HBM per device.

v0:
```python
import jax
import jax.numpy as jnp
from jax import lax
from jax.sharding import PartitionSpec as P

beta_one = 0.9
beta_two = 0.9
learn_rate = 0.01


def project_rows(factors, grads, local_width):
    high_part = grads.astype(jnp.bfloat16)
    low_part = (grads - high_part.astype(jnp.float32)).astype(jnp.bfloat16)
    outputs = []
    for member in range(3):
        lower = member * local_width
        upper = (member + 1) * local_width
        factor_t = factors[member].T
        first_term = jnp.dot(
            factor_t, high_part[:, lower:upper], preferred_element_type=jnp.float32
        )
        second_term = jnp.dot(
            factor_t, low_part[:, lower:upper], preferred_element_type=jnp.float32
        )
        outputs.append(first_term + second_term)
    return jnp.concatenate(outputs, axis=1)


def body(
    x_saved,
    h_saved,
    key_cot,
    value_cot,
    out_cot,
    w_key,
    w_value,
    w_out,
    p_key,
    p_value,
    p_out,
    m_key,
    m_value,
    m_out,
):
    local_width = key_cot.shape[1]
    x_cols = x_saved.T
    y_cols = out_cot.T
    grad_k = jnp.dot(x_cols, key_cot, preferred_element_type=jnp.float32)
    grad_v = jnp.dot(x_cols, value_cot, preferred_element_type=jnp.float32)
    grad_o = jnp.dot(y_cols, h_saved, preferred_element_type=jnp.float32)
    whole_grad = jnp.concatenate([grad_k, grad_v, grad_o], axis=1)
    partial_value = project_rows(
        (
            lax.all_gather(p_key, "fs", axis=0, tiled=True),
            lax.all_gather(p_value, "fs", axis=0, tiled=True),
            lax.all_gather(p_out, "fs", axis=0, tiled=True),
        ),
        whole_grad,
        local_width,
    )
    projected = lax.psum_scatter(partial_value, "fs", scatter_dimension=0, tiled=True)
    total = lax.psum(jnp.sum(projected * projected), ("fs", "tp"))
    entries = projected.size * lax.axis_size("fs") * lax.axis_size("tp")
    normed = projected / jnp.sqrt(total / entries + 1e-06)
    moments = jnp.concatenate([m_key, m_value, m_out], axis=2)
    moment_one = beta_one * moments[0] + (1 - beta_one) * normed
    moment_two = beta_two * moments[1] + (1 - beta_two) * normed * normed
    direction = (moment_one / jnp.sqrt(moment_two)).astype(jnp.bfloat16)
    gathered = lax.all_gather(direction, "fs", axis=0, tiled=True)
    step_key = jnp.dot(p_key, gathered[:, :local_width], preferred_element_type=jnp.float32)
    step_value = jnp.dot(
        p_value, gathered[:, local_width : 2 * local_width], preferred_element_type=jnp.float32
    )
    step_out = jnp.dot(p_out, gathered[:, 2 * local_width :], preferred_element_type=jnp.float32).T
    fresh_key = (w_key - learn_rate * step_key).astype(jnp.bfloat16)
    fresh_value = (w_value - learn_rate * step_value).astype(jnp.bfloat16)
    fresh_out = (w_out - learn_rate * step_out).astype(jnp.bfloat16)
    copy_key, copy_value, copy_out = (
        lax.all_gather(fresh_key, "fs", axis=0, tiled=True),
        lax.all_gather(fresh_value, "fs", axis=0, tiled=True),
        lax.all_gather(fresh_out, "fs", axis=1, tiled=True),
    )
    stacked = jnp.stack([moment_one, moment_two])
    new_m_key = stacked[:, :, :local_width]
    new_m_value = stacked[:, :, local_width : 2 * local_width]
    new_m_out = stacked[:, :, 2 * local_width :]
    return (
        step_key,
        step_value,
        step_out,
        copy_key,
        copy_value,
        copy_out,
        new_m_key,
        new_m_value,
        new_m_out,
    )


def solution(mesh):
    in_specs = (
        P("fs", None),
        P("fs", "tp"),
        P("fs", "tp"),
        P("fs", "tp"),
        P("fs", None),
        P("fs", "tp"),
        P("fs", "tp"),
        P("tp", "fs"),
        P("fs", None),
        P("fs", None),
        P("fs", None),
        P(None, "fs", "tp"),
        P(None, "fs", "tp"),
        P(None, "fs", "tp"),
    )
    out_specs = (
        P("fs", "tp"),
        P("fs", "tp"),
        P("tp", "fs"),
        P(None, "tp"),
        P(None, "tp"),
        P("tp", None),
        P(None, "fs", "tp"),
        P(None, "fs", "tp"),
        P(None, "fs", "tp"),
    )
    return jax.shard_map(body, mesh=mesh, in_specs=in_specs, out_specs=out_specs, check_vma=False)
```

profile of v0, /device:TPU:0, one launch (start us, length us, event | category | flops | bytes accessed | tf_op | source)
XLA Modules:
  0.0 409.5 jit_solution(15238596800766914783)
XLA Ops:
  9.5 5.9 %fusion.23 = f32[2048,256]{0,1:T(8,128)S(1)} fusion(bf16[2048,2048]{1,0:T(8,128)(2,1)} %param.14, bf16[2048,256]{1,0:T(8,128)(2,1)S(1)} %copy-done), kind=kOutput, calls=%fused_computation.47 | convolution fusion | flops 2147483648 | bytes 11534336 | tf_op jit(solution)/shard_map/dot_general | solution.py:48
  15.4 5.9 %fusion.24 = f32[2048,256]{0,1:T(8,128)S(1)} fusion(bf16[2048,2048]{1,0:T(8,128)(2,1)} %param.14, bf16[2048,256]{1,0:T(8,128)(2,1)S(1)} %copy-done.6), kind=kOutput, calls=%fused_computation.48 | convolution fusion | flops 2147483648 | bytes 11534336 | tf_op jit(solution)/shard_map/dot_general | solution.py:49
  21.4 2.4 fusion.25
  23.8 2.0 fusion
  25.8 2.1 subtract_convert_fusion
  27.8 25.3 %all-gather.7.cloned.1.call-done = bf16[2048,256]{1,0:T(8,128)(2,1)} async-done(((bf16[256,256]{1,0:T(8,128)(2,1)}), bf16[2048,256]{1,0:T(8,128)(2,1)}) %all-gather.7.cloned.1.call-update) | async-done | bytes 1048592 | tf_op jit(solution)/shard_map/all_gather | solution.py:54
  53.2 2.1 fusion.11
  55.2 39.1 %all-gather.9.cloned.1.call-done = bf16[2048,256]{1,0:T(8,128)(2,1)} async-done(((bf16[256,256]{1,0:T(8,128)(2,1)}), bf16[2048,256]{1,0:T(8,128)(2,1)}) %all-gather.9.cloned.1.call-update) | async-done | bytes 1048592 | tf_op jit(solution)/shard_map/all_gather | solution.py:55
  94.3 2.1 fusion.8
  98.1 1.7 fusion.2
  99.7 35.7 %all-gather.11.cloned.1.call-done = bf16[2048,256]{1,0:T(8,128)(2,1)} async-done(((bf16[256,256]{1,0:T(8,128)(2,1)}), bf16[2048,256]{1,0:T(8,128)(2,1)}) %all-gather.11.cloned.1.call-update) | async-done | bytes 1048592 | tf_op jit(solution)/shard_map/all_gather | solution.py:56
  135.5 2.0 fusion.5
  137.5 2.0 fusion.1
  141.2 61.6 %reduce-scatter.4.cloned.1.call-done = f32[32,768]{1,0:T(8,128)} async-done(((f32[256,768]{1,0:T(8,128)}), f32[32,768]{1,0:T(8,128)}) %reduce-scatter.4.cloned.1.call-update) | async-done | bytes 98320
  204.8 40.2 %psum.7 = f32[]{:T(128)} all-reduce(f32[]{:T(128)} %multiply_reduce_fusion), channel_id=1, replica_groups=mesh['fs'=8,'tp'=4] {'fs','tp'}, use_global_device_ids=true, to_apply=%region_2.0 | all-reduce | flops 1 | bytes 8 | tf_op jit(solution)/shard_map/psum | solution.py:62
  245.9 31.0 %all_gather.24 = bf16[256,768]{1,0:T(8,128)(2,1)S(1)} all-gather(bf16[32,768]{1,0:T(8,128)(2,1)S(1)} %copy.40), channel_id=1, replica_groups=mesh['fs'=8,'tp'=4] {'fs'}, dimensions={0}, use_global_device_ids=true | all-gather | bytes 442368 | tf_op jit(solution)/shard_map/all_gather | solution.py:69
  280.0 1.8 subtract_convert_fusion.2
  283.0 1.8 subtract_convert_fusion.3
  287.4 31.3 %all-gather.17.cloned.1.call-done = bf16[256,2048]{0,1:T(8,128)(2,1)} async-done(((bf16[256,256]{0,1:T(8,128)(2,1)}), bf16[256,2048]{0,1:T(8,128)(2,1)}) %all-gather.17.cloned.1.call-update) | async-done | bytes 1048592 | tf_op jit(solution)/shard_map/all_gather | solution.py:81
  318.8 2.3 copy.51
  321.0 38.4 %all-gather.15.cloned.1.call-done = bf16[2048,256]{0,1:T(8,128)(2,1)} async-done(((bf16[256,256]{0,1:T(8,128)(2,1)}), bf16[2048,256]{0,1:T(8,128)(2,1)}) %all-gather.15.cloned.1.call-update) | async-done | bytes 1048592 | tf_op jit(solution)/shard_map/all_gather | solution.py:80
  359.4 2.3 copy.50
  361.6 38.8 %all-gather.13.cloned.1.call-done = bf16[2048,256]{0,1:T(8,128)(2,1)} async-done(((bf16[256,256]{0,1:T(8,128)(2,1)}), bf16[2048,256]{0,1:T(8,128)(2,1)}) %all-gather.13.cloned.1.call-update) | async-done | bytes 1048592 | tf_op jit(solution)/shard_map/all_gather | solution.py:79
  400.4 2.3 copy.49
  (63 shorter events, 14.6 us)
Async XLA Ops:
  7.2 2.3 copy-start
  7.2 46.0 %all-gather.7.cloned.1.call-start = ((), (), s32[]{:S(2)}) async-start(), calls=%async_computation.1 | async-start | bytes 1179648 | tf_op jit(solution)/shard_map/all_gather | solution.py:54
  7.9 86.4 %all-gather.9.cloned.1.call-start = ((), (), s32[]{:S(2)}) async-start(), calls=%async_computation.2 | async-start | bytes 1179648 | tf_op jit(solution)/shard_map/all_gather | solution.py:55
  8.7 126.8 %all-gather.11.cloned.1.call-start = ((), (), s32[]{:S(2)}) async-start(), calls=%async_computation.3 | async-start | bytes 1179648 | tf_op jit(solution)/shard_map/all_gather | solution.py:56
  9.4 6.0 %copy-start.6 = (bf16[2048,256]{1,0:T(8,128)(2,1)S(1)}, bf16[2048,256]{1,0:T(8,128)(2,1)}, u32[]{:S(2)}) copy-start(bf16[2048,256]{1,0:T(8,128)(2,1)} %param.17) | copy-start | bytes 3145732
  9.4 193.5 %reduce-scatter.4.cloned.1.call-start = ((), (), s32[]{:S(2)}) async-start(), calls=%async_computation.7 | async-start | bytes 884736
  9.5 11.9 %slice-start = ((s8[8388608]{0:T(1024)(128)(4,1)}), s8[4194304]{0:T(1024)(128)(4,1)S(1)}, s32[]{:S(2)}) async-start(s8[8388608]{0:T(1024)(128)(4,1)} %bitcast.42), calls=%async_computation.8 | async-start | bytes 8388608
  15.4 5.9 %slice-start.1 = ((s8[8388608]{0:T(1024)(128)(4,1)}), s8[4194304]{0:T(1024)(128)(4,1)S(1)}, s32[]{:S(2)}) async-start(s8[8388608]{0:T(1024)(128)(4,1)} %bitcast.42), calls=%async_computation.9 | async-start | bytes 8388608
  15.4 5.9 %copy-start.7 = (bf16[2048,256]{1,0:T(8,128)(2,1)S(1)}, bf16[2048,256]{1,0:T(8,128)(2,1)}, u32[]{:S(2)}) copy-start(bf16[2048,256]{1,0:T(8,128)(2,1)} %param.15) | copy-start | bytes 3145732
  53.2 43.2 %copy-start.8 = (bf16[2048,256]{1,0:T(8,128)(2,1)S(1)}, bf16[2048,256]{1,0:T(8,128)(2,1)}, u32[]{:S(2)}) copy-start(bf16[2048,256]{1,0:T(8,128)(2,1)} %all-gather.7.cloned.1.call-done) | copy-start | bytes 3145732
  94.3 3.8 copy-start.9
  137.4 3.4 copy-start.3
  137.5 3.4 copy-start.4
  137.5 3.4 copy-start.5
  139.5 65.1 %copy-start.2 = (f32[256,256]{1,0:T(8,128)S(1)}, f32[256,256]{1,0:T(8,128)}, u32[]{:S(2)}) copy-start(f32[256,256]{1,0:T(8,128)} %param.21) | copy-start | bytes 786436
  140.8 178.0 %all-gather.17.cloned.1.call-start = ((), (), s32[]{:S(2)}) async-start(), calls=%async_computation.6 | async-start | bytes 1179648 | tf_op jit(solution)/shard_map/all_gather | solution.py:81
  278.0 8.7 %copy-start.1 = (f32[256,256]{1,0:T(8,128)}, f32[256,256]{1,0:T(8,128)S(1)}, u32[]{:S(2)}) copy-start(f32[256,256]{1,0:T(8,128)S(1)} %fusion.14) | copy-start | bytes 786436
  278.9 80.5 %all-gather.15.cloned.1.call-start = ((), (), s32[]{:S(2)}) async-start(), calls=%async_computation.5 | async-start | bytes 1179648 | tf_op jit(solution)/shard_map/all_gather | solution.py:80
  281.8 118.6 %all-gather.13.cloned.1.call-start = ((), (), s32[]{:S(2)}) async-start(), calls=%async_computation.4 | async-start | bytes 1179648 | tf_op jit(solution)/shard_map/all_gather | solution.py:79
Sparse Core Ops, SparseCore 0:
  10.1 42.9 all-gather.6
  55.3 38.9 all-gather.8
  96.4 38.9 all-gather.10
  140.9 61.9 reduce-scatter.3
  279.0 39.7 all-gather.16
  321.2 38.0 all-gather.14
  362.0 38.3 all-gather.12
where the time goes:
time: 410 us
  waiting for transfers between devices  272 us (66%)
  blocking collectives  71.1 us (17%)
  matrix products  30.3 us (7%)
  between operations  15.2 us (4%)
  local copies, waits for them, and re-layouts  13.9 us (3%)
  other arithmetic  6.34 us (2%)
    unnamed x8, waiting for transfers between devices  63.8 us
    psum x1, blocking collectives, body(): total = lax.psum(jnp.sum(projected * projected), ('fs', 'tp'))  40.2 us
    all_gather x1, waiting for transfers between devices, body(): lax.all_gather(p_value, 'fs', axis=0, tiled=True)  39.1 us
    all_gather x1, waiting for transfers between devices, body(): lax.all_gather(fresh_key, 'fs', axis=0, tiled=True)  38.8 us
    all_gather x1, waiting for transfers between devices, body(): lax.all_gather(fresh_value, 'fs', axis=0, tiled=True)  38.4 us
    all_gather x1, waiting for transfers between devices, body(): lax.all_gather(p_out, 'fs', axis=0, tiled=True)  35.7 us
    all_gather x1, waiting for transfers between devices, body(): lax.all_gather(fresh_out, 'fs', axis=1, tiled=True)  31.3 us
    all_gather x1, blocking collectives, body(): gathered = lax.all_gather(direction, 'fs', axis=0, tiled=True)  31 us
  transfers between devices with their start and end apart: 7, of which 7 were waited for; matrix products, arithmetic and copies ran while one was open for 10% of the time, Pallas kernels for 0%

commit v1 on v0

--- a/solution.py
+++ b/solution.py
@@ -66,7 +66,12 @@
     moment_one = beta_one * moments[0] + (1 - beta_one) * normed
     moment_two = beta_two * moments[1] + (1 - beta_two) * normed * normed
     direction = (moment_one / jnp.sqrt(moment_two)).astype(jnp.bfloat16)
-    gathered = lax.all_gather(direction, "fs", axis=0, tiled=True)
+    ring = [direction]
+    for hop in range(7):
+        ring.append(lax.ppermute(ring[-1], "fs", [(dev, (dev + 1) % 8) for dev in range(8)]))
+    gathered = jnp.roll(
+        jnp.concatenate(ring[::-1], axis=0), (lax.axis_index("fs") + 1) * ring[0].shape[0], axis=0
+    )
     step_key = jnp.dot(p_key, gathered[:, :local_width], preferred_element_type=jnp.float32)
     step_value = jnp.dot(
         p_value, gathered[:, local_width : 2 * local_width], preferred_element_type=jnp.float32

time: 410 us -> 446 us (1.088)
  waiting for transfers between devices: 272 us -> 330 us
  blocking collectives: 71.1 us -> 40.1 us
  local copies, waits for them, and re-layouts: 13.9 us -> 19.8 us
    ppermute x0 -> x7, waiting for transfers between devices: none -> 58.4 us  [body(): lax.ppermute(ring[-1], 'fs', [(dev, (dev + 1) % 8) for dev in range(8)])]
    all_gather x1 -> x0, blocking collectives: 31 us -> none  [body(): gathered = lax.all_gather(direction, 'fs', axis=0, tiled=True)]
    unnamed x38 -> x44, local copies, waits for them, and re-layouts: 13.4 us -> 15.5 us
  transfers between devices with their start and end apart: 7 -> 14, of which waited for: 7 -> 14; matrix products, arithmetic and copies ran while one was open for 10% -> 9% of each run, Pallas kernels for 0% -> 0%
where the time goes in v1:
time: 446 us; the launch traced here: 445 us
  waiting for transfers between devices  330 us (74%)
  blocking collectives  40.1 us (9%)
  matrix products  29.6 us (7%)
  local copies, waits for them, and re-layouts  19.8 us (4%)
  between operations  15.2 us (3%)
  other arithmetic  7.29 us (2%)
    unnamed x8, waiting for transfers between devices  63.9 us
    ppermute x7, waiting for transfers between devices, body(): lax.ppermute(ring[-1], 'fs', [(dev, (dev + 1) % 8) for dev in range(8)])  58.4 us
    psum x1, blocking collectives, body(): total = lax.psum(jnp.sum(projected * projected), ('fs', 'tp'))  40.1 us
    all_gather x1, waiting for transfers between devices, body(): lax.all_gather(p_value, 'fs', axis=0, tiled=True)  39.1 us
    all_gather x1, waiting for transfers between devices, body(): lax.all_gather(fresh_key, 'fs', axis=0, tiled=True)  38.8 us
    all_gather x1, waiting for transfers between devices, body(): lax.all_gather(fresh_value, 'fs', axis=0, tiled=True)  38.4 us
    all_gather x1, waiting for transfers between devices, body(): lax.all_gather(p_out, 'fs', axis=0, tiled=True)  35.7 us
    all_gather x1, waiting for transfers between devices, body(): lax.all_gather(fresh_out, 'fs', axis=1, tiled=True)  30.6 us
  transfers between devices with their start and end apart: 14, of which 14 were waited for; matrix products, arithmetic and copies ran while one was open for 9% of the time, Pallas kernels for 0%

profile of v1, /device:TPU:0, one launch (start us, length us, event | category | flops | bytes accessed | tf_op | source)
XLA Modules:
  0.0 444.9 jit_solution(16958204833958219884)
XLA Ops:
  9.5 5.8 %fusion.24 = f32[2048,256]{0,1:T(8,128)S(1)} fusion(bf16[2048,2048]{1,0:T(8,128)(2,1)} %param.14, bf16[2048,256]{1,0:T(8,128)(2,1)S(1)} %copy-done), kind=kOutput, calls=%fused_computation.48 | convolution fusion | flops 2147483648 | bytes 11534336 | tf_op jit(solution)/shard_map/dot_general | solution.py:48
  15.3 5.9 %fusion.25 = f32[2048,256]{0,1:T(8,128)S(1)} fusion(bf16[2048,2048]{1,0:T(8,128)(2,1)} %param.14, bf16[2048,256]{1,0:T(8,128)(2,1)S(1)} %copy-done.11), kind=kOutput, calls=%fused_computation.49 | convolution fusion | flops 2147483648 | bytes 11534336 | tf_op jit(solution)/shard_map/dot_general | solution.py:49
  21.4 2.4 fusion.26
  25.8 2.1 subtract_convert_fusion
  27.9 25.3 %all-gather.7.cloned.1.call-done = bf16[2048,256]{1,0:T(8,128)(2,1)} async-done(((bf16[256,256]{1,0:T(8,128)(2,1)}), bf16[2048,256]{1,0:T(8,128)(2,1)}) %all-gather.7.cloned.1.call-update) | async-done | bytes 1048592 | tf_op jit(solution)/shard_map/all_gather | solution.py:54
  55.2 39.1 %all-gather.9.cloned.1.call-done = bf16[2048,256]{1,0:T(8,128)(2,1)} async-done(((bf16[256,256]{1,0:T(8,128)(2,1)}), bf16[2048,256]{1,0:T(8,128)(2,1)}) %all-gather.9.cloned.1.call-update) | async-done | bytes 1048592 | tf_op jit(solution)/shard_map/all_gather | solution.py:55
  99.7 35.7 %all-gather.11.cloned.1.call-done = bf16[2048,256]{1,0:T(8,128)(2,1)} async-done(((bf16[256,256]{1,0:T(8,128)(2,1)}), bf16[2048,256]{1,0:T(8,128)(2,1)}) %all-gather.11.cloned.1.call-update) | async-done | bytes 1048592 | tf_op jit(solution)/shard_map/all_gather | solution.py:56
  141.1 61.8 %reduce-scatter.4.cloned.1.call-done = f32[32,768]{1,0:T(8,128)} async-done(((f32[256,768]{1,0:T(8,128)}), f32[32,768]{1,0:T(8,128)}) %reduce-scatter.4.cloned.1.call-update) | async-done | bytes 98320
  204.8 40.1 %psum.7 = f32[]{:T(128)} all-reduce(f32[]{:T(128)} %multiply_reduce_fusion), channel_id=1, replica_groups=mesh['fs'=8,'tp'=4] {'fs','tp'}, use_global_device_ids=true, to_apply=%region_2.0 | all-reduce | flops 1 | bytes 8 | tf_op jit(solution)/shard_map/psum | solution.py:62
  245.7 2.5 collective-permute-start
  248.3 6.2 %collective-permute-done = bf16[32,768]{0,1:T(8,128)(2,1)S(1)} collective-permute-done((bf16[32,768]{0,1:T(8,128)(2,1)S(1)}, bf16[32,768]{0,1:T(8,128)(2,1)S(1)}, u32[]{:S(2)}, u32[]{:S(2)}) %collective-permute-start) | collective-permute-done | bytes 49184 | tf_op jit(solution)/shard_map/ppermute | solution.py:71
  254.5 8.4 %collective-permute-done.1 = bf16[32,768]{0,1:T(8,128)(2,1)S(1)} collective-permute-done((bf16[32,768]{0,1:T(8,128)(2,1)S(1)}, bf16[32,768]{0,1:T(8,128)(2,1)S(1)}, u32[]{:S(2)}, u32[]{:S(2)}) %collective-permute-start.1) | collective-permute-done | bytes 49184 | tf_op jit(solution)/shard_map/ppermute | solution.py:71
  262.9 8.4 %collective-permute-done.2 = bf16[32,768]{0,1:T(8,128)(2,1)S(1)} collective-permute-done((bf16[32,768]{0,1:T(8,128)(2,1)S(1)}, bf16[32,768]{0,1:T(8,128)(2,1)S(1)}, u32[]{:S(2)}, u32[]{:S(2)}) %collective-permute-start.2) | collective-permute-done | bytes 49184 | tf_op jit(solution)/shard_map/ppermute | solution.py:71
  271.2 8.4 %collective-permute-done.3 = bf16[32,768]{0,1:T(8,128)(2,1)S(1)} collective-permute-done((bf16[32,768]{0,1:T(8,128)(2,1)S(1)}, bf16[32,768]{0,1:T(8,128)(2,1)S(1)}, u32[]{:S(2)}, u32[]{:S(2)}) %collective-permute-start.3) | collective-permute-done | bytes 49184 | tf_op jit(solution)/shard_map/ppermute | solution.py:71
  279.6 9.3 %collective-permute-done.4 = bf16[32,768]{0,1:T(8,128)(2,1)S(1)} collective-permute-done((bf16[32,768]{0,1:T(8,128)(2,1)S(1)}, bf16[32,768]{0,1:T(8,128)(2,1)S(1)}, u32[]{:S(2)}, u32[]{:S(2)}) %collective-permute-start.4) | collective-permute-done | bytes 49184 | tf_op jit(solution)/shard_map/ppermute | solution.py:71
  288.9 10.5 %collective-permute-done.5 = bf16[32,768]{0,1:T(8,128)(2,1)S(1)} collective-permute-done((bf16[32,768]{0,1:T(8,128)(2,1)S(1)}, bf16[32,768]{0,1:T(8,128)(2,1)S(1)}, u32[]{:S(2)}, u32[]{:S(2)}) %collective-permute-start.5) | collective-permute-done | bytes 49184 | tf_op jit(solution)/shard_map/ppermute | solution.py:71
  300.6 7.3 %collective-permute-done.6 = bf16[32,768]{0,1:T(8,128)(2,1)} collective-permute-done((bf16[32,768]{0,1:T(8,128)(2,1)S(1)}, bf16[32,768]{0,1:T(8,128)(2,1)}, u32[]{:S(2)}, u32[]{:S(2)}) %collective-permute-start.6) | collective-permute-done | bytes 49184 | tf_op jit(solution)/shard_map/ppermute | solution.py:71
  307.9 3.2 concatenate.18
  323.5 30.6 %all-gather.17.cloned.1.call-done = bf16[256,2048]{0,1:T(8,128)(2,1)} async-done(((bf16[256,256]{0,1:T(8,128)(2,1)}), bf16[256,2048]{0,1:T(8,128)(2,1)}) %all-gather.17.cloned.1.call-update) | async-done | bytes 1048592 | tf_op jit(solution)/shard_map/all_gather | solution.py:86
  354.1 2.3 copy.50
  356.4 38.4 %all-gather.15.cloned.1.call-done = bf16[2048,256]{0,1:T(8,128)(2,1)} async-done(((bf16[256,256]{0,1:T(8,128)(2,1)}), bf16[2048,256]{0,1:T(8,128)(2,1)}) %all-gather.15.cloned.1.call-update) | async-done | bytes 1048592 | tf_op jit(solution)/shard_map/all_gather | solution.py:85
  394.8 2.3 copy.49
  397.0 38.8 %all-gather.13.cloned.1.call-done = bf16[2048,256]{0,1:T(8,128)(2,1)} async-done(((bf16[256,256]{0,1:T(8,128)(2,1)}), bf16[2048,256]{0,1:T(8,128)(2,1)}) %all-gather.13.cloned.1.call-update) | async-done | bytes 1048592 | tf_op jit(solution)/shard_map/all_gather | solution.py:84
  435.8 2.3 copy.48
  (81 shorter events, 32.9 us)
Async XLA Ops:
  7.2 46.0 %all-gather.7.cloned.1.call-start = ((), (), s32[]{:S(2)}) async-start(), calls=%async_computation.1 | async-start | bytes 1179648 | tf_op jit(solution)/shard_map/all_gather | solution.py:54
  7.9 86.4 %all-gather.9.cloned.1.call-start = ((), (), s32[]{:S(2)}) async-start(), calls=%async_computation.2 | async-start | bytes 1179648 | tf_op jit(solution)/shard_map/all_gather | solution.py:55
  8.7 126.8 %all-gather.11.cloned.1.call-start = ((), (), s32[]{:S(2)}) async-start(), calls=%async_computation.3 | async-start | bytes 1179648 | tf_op jit(solution)/shard_map/all_gather | solution.py:56
  9.4 5.9 %copy-start.11 = (bf16[2048,256]{1,0:T(8,128)(2,1)S(1)}, bf16[2048,256]{1,0:T(8,128)(2,1)}, u32[]{:S(2)}) copy-start(bf16[2048,256]{1,0:T(8,128)(2,1)} %param.17) | copy-start | bytes 3145732
  9.4 193.5 %reduce-scatter.4.cloned.1.call-start = ((), (), s32[]{:S(2)}) async-start(), calls=%async_computation.7 | async-start | bytes 884736
  15.3 5.9 %copy-start.10 = (bf16[2048,2048]{1,0:T(8,128)(2,1)S(1)}, bf16[2048,2048]{1,0:T(8,128)(2,1)}, u32[]{:S(2)}) copy-start(bf16[2048,2048]{1,0:T(8,128)(2,1)} %param.18) | copy-start | bytes 25165828
  15.3 6.1 %copy-start.12 = (bf16[2048,256]{1,0:T(8,128)(2,1)S(1)}, bf16[2048,256]{1,0:T(8,128)(2,1)}, u32[]{:S(2)}) copy-start(bf16[2048,256]{1,0:T(8,128)(2,1)} %param.15) | copy-start | bytes 3145732
  53.2 43.2 %copy-start.13 = (bf16[2048,256]{1,0:T(8,128)(2,1)S(1)}, bf16[2048,256]{1,0:T(8,128)(2,1)}, u32[]{:S(2)}) copy-start(bf16[2048,256]{1,0:T(8,128)(2,1)} %all-gather.7.cloned.1.call-done) | copy-start | bytes 3145732
  94.3 3.8 copy-start.14
  140.8 213.4 %all-gather.17.cloned.1.call-start = ((), (), s32[]{:S(2)}) async-start(), calls=%async_computation.6 | async-start | bytes 1179648 | tf_op jit(solution)/shard_map/all_gather | solution.py:86
  245.7 8.8 %collective-permute-start = (bf16[32,768]{0,1:T(8,128)(2,1)S(1)}, bf16[32,768]{0,1:T(8,128)(2,1)S(1)}, u32[]{:S(2)}, u32[]{:S(2)}) collective-permute-start(bf16[32,768]{0,1:T(8,128)(2,1)S(1)} %get-tuple-element.28), channel_id=1, source_target_pairs={{0,4},{4,8},{8,12},{12,16},{16,20},{20,24},{24,28},{28,0},{1,5},{5... | collective-permute-start | bytes 147464 | tf_op jit(solution)/shard_map/ppermute | solution.py:71
  254.5 8.4 %collective-permute-start.1 = (bf16[32,768]{0,1:T(8,128)(2,1)S(1)}, bf16[32,768]{0,1:T(8,128)(2,1)S(1)}, u32[]{:S(2)}, u32[]{:S(2)}) collective-permute-start(bf16[32,768]{0,1:T(8,128)(2,1)S(1)} %collective-permute-done), channel_id=1, source_target_pairs={{0,4},{4,8},{8,12},{12,16},{16,20},{20,24},{24,28},{28,0},{1,5},{5... | collective-permute-start | bytes 147464 | tf_op jit(solution)/shard_map/ppermute | solution.py:71
  262.9 8.4 %collective-permute-start.2 = (bf16[32,768]{0,1:T(8,128)(2,1)S(1)}, bf16[32,768]{0,1:T(8,128)(2,1)S(1)}, u32[]{:S(2)}, u32[]{:S(2)}) collective-permute-start(bf16[32,768]{0,1:T(8,128)(2,1)S(1)} %collective-permute-done.1), channel_id=1, source_target_pairs={{0,4},{4,8},{8,12},{12,16},{16,20},{20,24},{24,28},{28,0},{1,5},{5... | collective-permute-start | bytes 147464 | tf_op jit(solution)/shard_map/ppermute | solution.py:71
  271.2 28.2 %copy-start.2 = (bf16[32,768]{0,1:T(8,128)(2,1)}, bf16[32,768]{0,1:T(8,128)(2,1)S(1)}, u32[]{:S(2)}) copy-start(bf16[32,768]{0,1:T(8,128)(2,1)S(1)} %collective-permute-done.2) | copy-start | bytes 147460
  271.2 8.4 %collective-permute-start.3 = (bf16[32,768]{0,1:T(8,128)(2,1)S(1)}, bf16[32,768]{0,1:T(8,128)(2,1)S(1)}, u32[]{:S(2)}, u32[]{:S(2)}) collective-permute-start(bf16[32,768]{0,1:T(8,128)(2,1)S(1)} %collective-permute-done.2), channel_id=1, source_target_pairs={{0,4},{4,8},{8,12},{12,16},{16,20},{20,24},{24,28},{28,0},{1,5},{5... | collective-permute-start | bytes 147464 | tf_op jit(solution)/shard_map/ppermute | solution.py:71
  279.6 21.0 %copy-start.3 = (bf16[32,768]{0,1:T(8,128)(2,1)}, bf16[32,768]{0,1:T(8,128)(2,1)S(1)}, u32[]{:S(2)}) copy-start(bf16[32,768]{0,1:T(8,128)(2,1)S(1)} %collective-permute-done.3) | copy-start | bytes 147460
  279.6 9.3 %collective-permute-start.4 = (bf16[32,768]{0,1:T(8,128)(2,1)S(1)}, bf16[32,768]{0,1:T(8,128)(2,1)S(1)}, u32[]{:S(2)}, u32[]{:S(2)}) collective-permute-start(bf16[32,768]{0,1:T(8,128)(2,1)S(1)} %collective-permute-done.3), channel_id=1, source_target_pairs={{0,4},{4,8},{8,12},{12,16},{16,20},{20,24},{24,28},{28,0},{1,5},{5... | collective-permute-start | bytes 147464 | tf_op jit(solution)/shard_map/ppermute | solution.py:71
  288.9 11.7 %copy-start.4 = (bf16[32,768]{0,1:T(8,128)(2,1)}, bf16[32,768]{0,1:T(8,128)(2,1)S(1)}, u32[]{:S(2)}) copy-start(bf16[32,768]{0,1:T(8,128)(2,1)S(1)} %collective-permute-done.4) | copy-start | bytes 147460
  288.9 10.5 %collective-permute-start.5 = (bf16[32,768]{0,1:T(8,128)(2,1)S(1)}, bf16[32,768]{0,1:T(8,128)(2,1)S(1)}, u32[]{:S(2)}, u32[]{:S(2)}) collective-permute-start(bf16[32,768]{0,1:T(8,128)(2,1)S(1)} %collective-permute-done.4), channel_id=1, source_target_pairs={{0,4},{4,8},{8,12},{12,16},{16,20},{20,24},{24,28},{28,0},{1,5},{5... | collective-permute-start | bytes 147464 | tf_op jit(solution)/shard_map/ppermute | solution.py:71
  299.4 8.5 %collective-permute-start.6 = (bf16[32,768]{0,1:T(8,128)(2,1)S(1)}, bf16[32,768]{0,1:T(8,128)(2,1)}, u32[]{:S(2)}, u32[]{:S(2)}) collective-permute-start(bf16[32,768]{0,1:T(8,128)(2,1)S(1)} %collective-permute-done.5), channel_id=1, source_target_pairs={{0,4},{4,8},{8,12},{12,16},{16,20},{20,24},{24,28},{28,0},{1,5},{5... | collective-permute-start | bytes 147464 | tf_op jit(solution)/shard_map/ppermute | solution.py:71
  311.1 7.9 %copy-start.6 = (bf16[256,256]{1,0:T(8,128)(2,1)S(1)}, bf16[256,256]{1,0:T(8,128)(2,1)}, u32[]{:S(2)}) copy-start(bf16[256,256]{1,0:T(8,128)(2,1)} %param.22) | copy-start | bytes 393220
  312.3 5.6 %copy-start.1 = (f32[256,256]{1,0:T(8,128)}, f32[256,256]{1,0:T(8,128)S(1)}, u32[]{:S(2)}) copy-start(f32[256,256]{1,0:T(8,128)S(1)} %fusion.14) | copy-start | bytes 786436
  314.8 80.0 %all-gather.15.cloned.1.call-start = ((), (), s32[]{:S(2)}) async-start(), calls=%async_computation.5 | async-start | bytes 1179648 | tf_op jit(solution)/shard_map/all_gather | solution.py:85
  317.9 118.0 %all-gather.13.cloned.1.call-start = ((), (), s32[]{:S(2)}) async-start(), calls=%async_computation.4 | async-start | bytes 1179648 | tf_op jit(solution)/shard_map/all_gather | solution.py:84
  (5 other events, 13.6 us)
Sparse Core Ops, SparseCore 0:
  10.1 42.9 all-gather.6
  55.3 38.9 all-gather.8
  96.4 38.9 all-gather.10
  140.9 61.9 reduce-scatter.3
  314.9 39.1 all-gather.16
  356.6 38.0 all-gather.14
  397.4 38.3 all-gather.12
